TPU v7x, 32 devices: a whole 2x2x4 slice. The times are simulated.
32 devices in a mesh: ep: 8 (over z, y), tp: 4 (over x, core).
Axes of the slice: x: 2, y: 2, z: 4, core: 2. Of those that a mesh axis runs over, the one named last changes fastest.
Arguments:
- q_heads: bfloat16 [8192, 1024], P('ep', 'tp'), may hold values from -200 to 200
- k_heads: bfloat16 [8192, 256], P('ep', 'tp'), may hold values from -6 to 6
- v_heads: bfloat16 [8192, 256], P('ep', 'tp'), may hold values from -6 to 6
- sink_logits: float32 [16], P('tp'), may hold values from 1 to 5
- out_weight: bfloat16 [1024, 2048], P(None, 'tp'), may hold values from -1.5 to 1.5
- tokens_b: bfloat16 [4096, 2048], P('ep'), may hold values from -6 to 6
- moe_gain: float32 [2048], replicated, may hold values from 0.1 to 1.9
- router_group: bfloat16 [2048, 4], replicated, may hold values from -0.125 to 0.125
- router_expert: bfloat16 [2048, 16], replicated, may hold values from -0.125 to 0.125
- route_expert: int32 [4096, 2], P('ep'), may hold values from 0 to 15, as said below
- expert_gate: bfloat16 [16, 2048, 1024], P('ep', None, 'tp'), may hold values from -0.125 to 0.125
- expert_up: bfloat16 [16, 2048, 1024], P('ep', None, 'tp'), may hold values from -0.125 to 0.125
- expert_down: bfloat16 [16, 1024, 2048], P('ep', 'tp'), may hold values from -0.75 to 0.75
Outputs:
- mixer_out: bfloat16 [8192, 2048], P('ep', 'tp')
- moe_out: bfloat16 [4096, 2048], P(('ep', 'tp'))
Inputs may be any that keep to these rules, and one draw needn't show every extreme that they name: `route_expert`: each token names two different experts, in rising order, of one group of 4 consecutive experts. In each aligned block of 128 rows (the rows of one device) no expert is named by more than 32 tokens, in each group one expert is named by exactly 32 tokens of every block, and each group is named by a quarter of every block's tokens.
All inputs are finite; a program needn't handle non-finite values.
Results may differ from a plain program's by a relative error of at most 0.011.
Values may be sent and summed in bfloat16 or wider, within the bound.
No kernel may reach another device: no remote copies, remote signals or barrier semaphores. Data moves between devices by JAX's collectives and lax.ppermute only.
A program may use at most 128 MiB of HBM per device.

v0:
```python
import jax
import jax.numpy as jnp
from jax import lax
from jax.sharding import PartitionSpec as P

HEADS = 16
KV = 4
HD = 64
WINDOW = 128


def shifted(value, axis, steps):
    count = lax.axis_size(axis)
    leading, last = (max(0, -steps), min(count, count - steps))
    return lax.ppermute(value, axis, [(source, source + steps) for source in range(leading, last)])


def normalize(rows_in, gain):
    values = rows_in.astype(jnp.float32)
    scaled = values * lax.rsqrt(jnp.mean(values * values, axis=-1, keepdims=True) + 1e-06) * gain
    return scaled.astype(jnp.bfloat16)


def gate_weights(normed, routes, router_group, router_expert):
    group_logits = jnp.dot(normed, router_group, preferred_element_type=jnp.float32)
    expert_logits = jnp.dot(normed, router_expert, preferred_element_type=jnp.float32)
    group_count = router_group.shape[1]
    expert_count = router_expert.shape[1]
    chosen_group = routes[:, 0] // (expert_count // group_count)
    group_match = chosen_group[:, None] == jnp.arange(group_count, dtype=jnp.int32)[None, :]
    group_share = jnp.sum(
        jnp.where(group_match, jax.nn.softmax(group_logits, axis=-1), 0.0), axis=-1
    )
    expert_match = routes[:, :, None] == jnp.arange(expert_count, dtype=jnp.int32)[None, None, :]
    picked = jnp.sum(jnp.where(expert_match, expert_logits[:, None, :], 0.0), axis=-1)
    return group_share[:, None] * jax.nn.softmax(picked, axis=-1)


def slot_positions(routes, sub_count, expert_count):
    flat_routes = routes.reshape(sub_count, -1)
    onehot = (
        flat_routes[:, :, None] == jnp.arange(expert_count, dtype=jnp.int32)[None, None, :]
    ).astype(jnp.int32)
    places = jnp.sum(onehot * jnp.cumsum(onehot, axis=1), axis=2) - 1
    return (flat_routes, places)


def fill_slots(normed, flat_routes, places, sub_count, expert_count, capacity, exp_local):
    sub_index = jnp.arange(sub_count, dtype=jnp.int32)[:, None]
    target = ((flat_routes * sub_count + sub_index) * capacity + places).reshape(-1)
    source = jnp.repeat(normed, 2, axis=0)
    buffer = jnp.zeros((expert_count * sub_count * capacity, normed.shape[1]), jnp.bfloat16)
    buffer = buffer.at[target].set(source)
    return buffer.reshape(
        expert_count // exp_local, exp_local, sub_count, capacity, normed.shape[1]
    )


def per_device(
    q_heads,
    k_heads,
    v_heads,
    sink_logits,
    out_weight,
    tokens_b,
    moe_gain,
    router_group,
    router_expert,
    route_expert,
    expert_gate,
    expert_up,
    expert_down,
):
    span_len = WINDOW
    row_count = q_heads.shape[0]
    kv_local = k_heads.shape[1] // HD
    group_size = HEADS // KV
    blocks = row_count // span_len
    stacked = jnp.stack([k_heads[row_count - span_len :], v_heads[row_count - span_len :]])
    earlier = shifted(stacked, "ep", 1)

    def make_band(own_rows, prev_rows):
        extended = jnp.concatenate([prev_rows, own_rows], axis=0).reshape(
            blocks + 1, span_len, kv_local, HD
        )
        return jnp.concatenate([extended[:-1], extended[1:]], axis=1)

    key_band = make_band(k_heads, earlier[0])
    value_band = make_band(v_heads, earlier[1])
    query_blocks = q_heads.reshape(blocks, span_len, kv_local, group_size, HD)
    scores = jnp.einsum(
        "nqhgd,nkhd->nhgqk", query_blocks, key_band, preferred_element_type=jnp.float32
    ) * HD ** (-0.5)
    first_row = lax.axis_index("ep") * row_count
    query_index = jnp.arange(span_len, dtype=jnp.int32)[:, None]
    key_index = jnp.arange(2 * span_len, dtype=jnp.int32)[None, :]
    distance = query_index + span_len - key_index
    key_place = (
        first_row
        + jnp.arange(blocks, dtype=jnp.int32)[:, None, None] * span_len
        + key_index[None]
        - span_len
    )
    allowed = (distance >= 0)[None] & (distance < span_len)[None] & (key_place >= 0)
    masked = jnp.where(allowed[:, None, None], scores, -1e30)
    sink_full = sink_logits.reshape(kv_local, group_size)[None, :, :, None]
    row_max = jnp.maximum(jnp.max(masked, axis=-1), sink_full)
    weights_exp = jnp.exp(masked - row_max[..., None])
    denominator = jnp.sum(weights_exp, axis=-1) + jnp.exp(sink_full - row_max)
    probs = (weights_exp / denominator[..., None]).astype(jnp.bfloat16)
    attended = jnp.einsum(
        "nhgqk,nkhd->nqhgd", probs, value_band, preferred_element_type=jnp.float32
    )
    attended = attended.astype(jnp.bfloat16).reshape(row_count, kv_local * group_size * HD)
    mixed = jnp.dot(
        lax.all_gather(attended, "tp", axis=1, tiled=True),
        out_weight,
        preferred_element_type=jnp.float32,
    )
    mixer_out = mixed.astype(jnp.bfloat16)
    tp_count = lax.axis_size("tp")
    tp_index = lax.axis_index("tp")
    exp_local = expert_gate.shape[0]
    expert_count = exp_local * lax.axis_size("ep")
    rows_dev = tokens_b.shape[0] // tp_count
    capacity = min(4 * rows_dev // expert_count, rows_dev // 4)
    own_routes = lax.dynamic_slice_in_dim(route_expert, tp_index * rows_dev, rows_dev, 0)
    own_normed = normalize(
        lax.dynamic_slice_in_dim(tokens_b, tp_index * rows_dev, rows_dev, 0), moe_gain
    )
    flat_routes, places = slot_positions(own_routes, 1, expert_count)
    buffer = fill_slots(own_normed, flat_routes, places, 1, expert_count, capacity, exp_local)
    delivered = lax.all_to_all(buffer, "ep", split_axis=0, concat_axis=0, tiled=True)
    arrived = lax.all_gather(delivered, "tp", axis=2, tiled=True)
    own_flat = flat_routes[0]
    own_places = places[0]
    gates = gate_weights(own_normed, own_routes, router_group, router_expert)
    gate_pre = jnp.einsum(
        "setcd,edf->setcf", arrived, expert_gate, preferred_element_type=jnp.float32
    )
    up_pre = jnp.einsum("setcd,edf->setcf", arrived, expert_up, preferred_element_type=jnp.float32)
    activated = (jax.nn.silu(gate_pre) * up_pre).astype(jnp.bfloat16)
    partial_value = jnp.einsum(
        "setcf,efd->setcd", activated, expert_down, preferred_element_type=jnp.float32
    )
    summed = lax.psum_scatter(
        partial_value.astype(jnp.bfloat16), "tp", scatter_dimension=2, tiled=True
    )
    returned = lax.all_to_all(summed, "ep", split_axis=0, concat_axis=0, tiled=True)
    returned = returned.reshape(expert_count * capacity, returned.shape[-1])
    picked_rows = returned[own_flat * capacity + own_places].reshape(
        rows_dev, 2, returned.shape[-1]
    )
    moe_out = jnp.sum(gates[:, :, None] * picked_rows.astype(jnp.float32), axis=1).astype(
        jnp.bfloat16
    )
    return (mixer_out, moe_out)


def solution(mesh):
    in_specs = (
        P("ep", "tp"),
        P("ep", "tp"),
        P("ep", "tp"),
        P("tp"),
        P(None, "tp"),
        P("ep", None),
        P(),
        P(),
        P(),
        P("ep", None),
        P("ep", None, "tp"),
        P("ep", None, "tp"),
        P("ep", "tp", None),
    )
    out_specs = (P("ep", "tp"), P(("ep", "tp"), None))
    return jax.shard_map(
        per_device, mesh=mesh, in_specs=in_specs, out_specs=out_specs, check_vma=False
    )
```

profile of v0, /device:TPU:0, one launch (start us, length us, event | category | flops | bytes accessed | tf_op | source)
XLA Modules:
  0.0 384.7 jit_solution(17518008943013169215)
XLA Ops:
  7.2 0.8 broadcast_multiply_fusion
  8.3 0.6 reduce-window.6
  9.7 1.2 fusion.24
  10.9 1.3 fusion.26
  12.2 1.6 broadcast_in_dim.34
  13.8 2.3 reshape.383
  16.0 4.4 %scatter_custom_fusion = bf16[512,2048]{1,0:T(8,128)(2,1)} fusion(s32[256]{0:T(256)S(1)} %bitcast.171, bf16[256,2048]{1,0:T(8,128)(2,1)} %reshape.383, bf16[]{:T(256)} %constant.67.clone.1), kind=kCustom, calls=%fused_computation.35 | custom fusion | bytes 2097664 | tf_op jit(solution)/shard_map/scatter | solution.py:53
  20.5 55.5 %all_to_all.10 = bf16[8,2,1,32,2048]{4,3,2,1,0:T(8,128)(2,1)S(1)} all-to-all(bf16[8,2,1,32,2048]{4,3,2,1,0:T(8,128)(2,1)} %bitcast.159), channel_id=1, replica_groups=mesh['ep'=8,'tp'=4] {'ep'}, dimensions={0} | all-to-all | bytes 4194304 | tf_op jit(solution)/shard_map/all_to_all | solution.py:133
  76.0 1.5 copy.69
  77.6 57.4 %all-gather.5.cloned.1.call-done = bf16[8,2,4,32,2048]{4,3,2,0,1:T(8,128)(2,1)} async-done(((bf16[8,2,1,32,2048]{4,3,2,0,1:T(8,128)(2,1)}), bf16[8,2,4,32,2048]{4,3,2,0,1:T(8,128)(2,1)}) %all-gather.5.cloned.1.call-update) | async-done | bytes 8388624 | tf_op jit(solution)/shard_map/all_gather | solution.py:134
  134.9 7.7 %fusion.3 = f32[2,8,4,32,256]{4,3,2,1,0:T(8,128)} fusion(bf16[8,2,4,32,2048]{4,3,2,0,1:T(8,128)(2,1)} %all-gather.5.cloned.1.call-done, bf16[2,2048,256]{2,1,0:T(8,128)(2,1)} %param.24), kind=kOutput, calls=%fused_computation.9 | convolution fusion | flops 2147483648 | bytes 12582912 | tf_op jit(solution)/shard_map/setcd,edf->setcf/dot_general | solution.py:141
  142.6 13.5 %convert_bitcast_fusion = bf16[8,2,4,32,2048]{4,3,2,0,1:T(8,128)(2,1)} fusion(bf16[2,256,2048]{2,1,0:T(8,128)(2,1)S(1)} %copy-done, f32[2,8,4,32,256]{4,3,2,1,0:T(8,128)} %fusion.3, bf16[8,2,4,32,2048]{4,3,2,0,1:T(8,128)(2,1)} %all-gather.5.cloned.1.call-done, bf16[2,2048,256]{2,1,0:T(8,128)(2,1)} %param.23), kind=kOutput, calls=%fused_computation.2 | convolution fusion | flops 4302307328 | bytes 23068672 | tf_op jit(solution)/shard_map/setcf,efd->setcd/dot_general | solution.py:143
  156.1 0.9 copy-done.3
  157.1 3.6 collective-permute-start
  161.2 0.4 reshape.392
  161.7 0.6 dynamic-slice
  162.5 0.9 fusion.1
  163.5 1.1 fusion
  164.5 0.8 copy-done.2
  165.4 143.8 %all-reduce.3.cloned.1.call-done = bf16[8,2,4,32,2048]{4,3,2,0,1:T(8,128)(2,1)} async-done(((bf16[8,2,4,32,2048]{4,3,2,0,1:T(8,128)(2,1)}), bf16[8,2,4,32,2048]{4,3,2,0,1:T(8,128)(2,1)}) %all-reduce.3.cloned.1.call-update) | async-done | bytes 8388624
  309.2 2.5 constant_dynamic-slice_fusion
  311.6 1.6 copy.70
  313.2 5.5 %all-to-all-start.1 = ((bf16[8,2,1,32,2048]{4,3,2,1,0:T(8,128)(2,1)}), bf16[8,2,1,32,2048]{4,3,2,1,0:T(8,128)(2,1)S(1)}, u32[]{:S(2)}, u32[]{:S(2)}) async-start(bf16[8,2,1,32,2048]{4,3,2,1,0:T(8,128)(2,1)} %copy.70), calls=%async_computation.1 | async-start | bytes 4194304 | tf_op jit(solution)/shard_map/all_to_all | solution.py:149
  318.8 3.4 fusion.21
  322.2 0.3 copy.61
  322.6 0.9 copy.91
  324.3 22.5 %all-gather.3.cloned.1.call-done = bf16[1024,1024]{0,1:T(8,128)(2,1)} async-done(((bf16[1024,256]{0,1:T(8,128)(2,1)}), bf16[1024,1024]{0,1:T(8,128)(2,1)}) %all-gather.3.cloned.1.call-update) | async-done | bytes 2097168 | tf_op jit(solution)/shard_map/all_gather | solution.py:116
  346.8 4.1 %convolution_convert_fusion = bf16[1024,512]{1,0:T(8,128)(2,1)} fusion(bf16[1024,1024]{0,1:T(8,128)(2,1)} %all-gather.3.cloned.1.call-done, bf16[1024,512]{1,0:T(8,128)(2,1)} %param.17), kind=kOutput, calls=%fused_computation.24 | convolution fusion | flops 1074266112 | bytes 4194304 | tf_op jit(solution)/shard_map/dot_general | solution.py:115
  350.9 15.8 %all-to-all-done.1 = bf16[8,2,1,32,2048]{4,3,2,1,0:T(8,128)(2,1)S(1)} async-done(((bf16[8,2,1,32,2048]{4,3,2,1,0:T(8,128)(2,1)}), bf16[8,2,1,32,2048]{4,3,2,1,0:T(8,128)(2,1)S(1)}, u32[]{:S(2)}, u32[]{:S(2)}) %all-to-all-start.1) | async-done | bytes 2097184 | tf_op jit(solution)/shard_map/all_to_all | solution.py:149
  366.7 2.3 gather_fusion
  369.0 3.5 reshape.370
  372.6 5.6 %multiply_reduce_fusion = bf16[128,2048]{1,0:T(8,128)(2,1)} fusion(f32[128,2,2048]{2,1,0:T(2,128)} %reshape.370, f32[128,2]{1,0:T(8,128)S(1)} %copy.62), kind=kLoop, calls=%fused_computation.22 | loop fusion | flops 786432 | bytes 2622464 | tf_op jit(solution)/shard_map/reduce_sum | solution.py:154
  (72 shorter events, 2.9 us)
Async XLA Ops:
  7.2 135.4 %copy-start = (bf16[2,256,2048]{2,1,0:T(8,128)(2,1)S(1)}, bf16[2,256,2048]{2,1,0:T(8,128)(2,1)}, u32[]{:S(2)}) copy-start(bf16[2,256,2048]{2,1,0:T(8,128)(2,1)} %param.25) | copy-start | bytes 6291460
  7.2 127.8 %all-gather.5.cloned.1.call-start = ((), (), s32[]{:S(2)}) async-start(), calls=%async_computation.3 | async-start | bytes 10485760 | tf_op jit(solution)/shard_map/all_gather | solution.py:134
  77.5 231.6 %all-reduce.3.cloned.1.call-start = ((), (), s32[]{:S(2)}) async-start(), calls=%async_computation.4 | async-start | bytes 16777216
  156.1 0.9 copy-start.3
  156.1 1.0 copy-start.4
  156.1 5.1 %copy-start.5 = (bf16[1024,256]{1,0:T(8,128)(2,1)S(1)}, bf16[1024,256]{1,0:T(8,128)(2,1)}, u32[]{:S(2)}) copy-start(bf16[1024,256]{1,0:T(8,128)(2,1)} %param.13) | copy-start | bytes 1572868
  157.1 4.6 %copy-start.9 = (u32[32]{0:T(128)S(1)}, u32[32]{0:T(128)}, u32[]{:S(2)}) copy-start(u32[32]{0:T(128)} %constant.75) | copy-start | bytes 388
  157.1 5.2 %collective-permute-start = (bf16[2,128,64]{1,2,0:T(8,128)(2,1)S(1)}, bf16[2,128,64]{1,2,0:T(8,128)(2,1)S(1)}, u32[]{:S(2)}, u32[]{:S(2)}) collective-permute-start(bf16[2,128,64]{1,2,0:T(8,128)(2,1)S(1)} %pad_maximum_fusion.2), channel_id=1, source_target_pairs={{0,4},{4,8},{8,12},{12,16},{16,20},{20,24},{24,28},{1,5},{5,9},{9,... | collective-permute-start | bytes 98312 | tf_op jit(solution)/shard_map/ppermute | solution.py:15
  162.5 0.9 copy-start.8
  163.4 1.9 copy-start.2
  313.2 53.4 %all-to-all-start.1 = ((bf16[8,2,1,32,2048]{4,3,2,1,0:T(8,128)(2,1)}), bf16[8,2,1,32,2048]{4,3,2,1,0:T(8,128)(2,1)S(1)}, u32[]{:S(2)}, u32[]{:S(2)}) async-start(bf16[8,2,1,32,2048]{4,3,2,1,0:T(8,128)(2,1)} %copy.70), calls=%async_computation.1 | async-start | bytes 4194304 | tf_op jit(solution)/shard_map/all_to_all | solution.py:149
  318.8 28.0 %all-gather.3.cloned.1.call-start = ((), (), s32[]{:S(2)}) async-start(), calls=%async_computation.2 | async-start | bytes 2621440 | tf_op jit(solution)/shard_map/all_gather | solution.py:116
  322.2 1.3 copy-start.6
  322.2 1.6 copy-start.7
  369.0 9.1 %copy-start.1 = (bf16[2,256,2048]{2,1,0:T(8,128)(2,1)S(1)}, bf16[2,256,2048]{2,1,0:T(8,128)(2,1)}, u32[]{:S(2)}) copy-start(bf16[2,256,2048]{2,1,0:T(8,128)(2,1)} %param.25) | copy-start | bytes 6291460
Sparse Core Ops, SparseCore 0:
  77.6 57.2 all-gather.4
  156.3 152.8 all-reduce.2
  323.6 23.1 all-gather.2
where the time goes:
time: 385 us
  waiting for transfers between devices  239 us (62%)
  blocking collectives  55.5 us (14%)
  matrix products  30.1 us (8%)
  local copies, waits for them, and re-layouts  24.9 us (6%)
  between operations  14.1 us (4%)
  other arithmetic  11.5 us (3%)
  starting transfers between devices  9.2 us (2%)
    unnamed x4, waiting for transfers between devices  144 us
    all_gather x1, waiting for transfers between devices, per_device(): arrived = lax.all_gather(delivered, 'tp', axis=2, tiled=True)  57.4 us
    all_to_all x1, blocking collectives, per_device(): lax.all_to_all(buffer, 'ep', split_axis=0, concat_axis=0, tiled=True)  55.5 us
    all_gather x1, waiting for transfers between devices, per_device(): lax.all_gather(attended, 'tp', axis=1, tiled=True)  22.5 us
    all_to_all x1, waiting for transfers between devices, per_device(): lax.all_to_all(summed, 'ep', split_axis=0, concat_axis=0, tiled=True)  15.8 us
    dot_general x1, matrix products, per_device(): jnp.einsum('setcf,efd->setcd', activated, expert_down, preferred_element_...  13.5 us
  transfers between devices with their start and end apart: 5, of which 4 were waited for; matrix products, arithmetic and copies ran while one was open for 3% of the time, Pallas kernels for 0%

commit v1 on v0

--- a/solution.py
+++ b/solution.py
@@ -131,7 +131,7 @@
     flat_routes, places = slot_positions(own_routes, 1, expert_count)
     buffer = fill_slots(own_normed, flat_routes, places, 1, expert_count, capacity, exp_local)
     delivered = lax.all_to_all(buffer, "ep", split_axis=0, concat_axis=0, tiled=True)
-    arrived = lax.all_gather(delivered, "tp", axis=2, tiled=True)
+    arrived = jnp.concatenate(lax.all_gather(delivered, "tp"), axis=2)
     own_flat = flat_routes[0]
     own_places = places[0]
     gates = gate_weights(own_normed, own_routes, router_group, router_expert)

time: 385 us -> 387 us (level)
  transfers between devices with their start and end apart: 5 -> 5, of which waited for: 4 -> 4; matrix products, arithmetic and copies ran while one was open for 3% -> 4% of each run, Pallas kernels for 0% -> 0%
where the time goes in v1:
time: 387 us; the launch traced here: 386 us
  waiting for transfers between devices  236 us (61%)
  blocking collectives  55.6 us (14%)
  matrix products  31.3 us (8%)
  local copies, waits for them, and re-layouts  28.3 us (7%)
  between operations  14.1 us (4%)
  other arithmetic  11.5 us (3%)
  starting transfers between devices  9.19 us (2%)
    unnamed x4, waiting for transfers between devices  140 us
    all_gather x1, waiting for transfers between devices, per_device(): arrived = jnp.concatenate(lax.all_gather(delivered, 'tp'), axis=2)  57.4 us
    all_to_all x1, blocking collectives, per_device(): lax.all_to_all(buffer, 'ep', split_axis=0, concat_axis=0, tiled=True)  55.6 us
    all_gather x1, waiting for transfers between devices, per_device(): lax.all_gather(attended, 'tp', axis=1, tiled=True)  22.5 us
    all_to_all x1, waiting for transfers between devices, per_device(): lax.all_to_all(summed, 'ep', split_axis=0, concat_axis=0, tiled=True)  15.9 us
    dot_general x1, matrix products, per_device(): jnp.einsum('setcf,efd->setcd', activated, expert_down, preferred_element_...  13.5 us
  transfers between devices with their start and end apart: 5, of which 4 were waited for; matrix products, arithmetic and copies ran while one was open for 4% of the time, Pallas kernels for 0%

profile of v1, /device:TPU:0, one launch (start us, length us, event | category | flops | bytes accessed | tf_op | source)
XLA Modules:
  0.0 385.9 jit_solution(6763377471499878188)
XLA Ops:
  7.2 0.8 broadcast_multiply_fusion
  8.3 0.6 reduce-window.6
  9.7 1.2 fusion.32
  10.9 1.3 fusion.34
  12.2 1.6 broadcast_in_dim.34
  13.8 2.3 reshape.391
  16.0 4.4 %scatter_custom_fusion = bf16[512,2048]{1,0:T(8,128)(2,1)} fusion(s32[256]{0:T(256)S(1)} %bitcast.180, bf16[256,2048]{1,0:T(8,128)(2,1)} %reshape.391, bf16[]{:T(256)} %constant.67.clone.1), kind=kCustom, calls=%fused_computation.39 | custom fusion | bytes 2097664 | tf_op jit(solution)/shard_map/scatter | solution.py:53
  20.5 55.6 %all_to_all.10 = bf16[8,2,1,32,2048]{4,3,1,2,0:T(8,128)(2,1)} all-to-all(bf16[8,2,1,32,2048]{4,3,1,2,0:T(8,128)(2,1)} %bitcast.168), channel_id=1, replica_groups=mesh['ep'=8,'tp'=4] {'ep'}, dimensions={0} | all-to-all | bytes 4194304 | tf_op jit(solution)/shard_map/all_to_all | solution.py:133
  76.2 57.4 %all-gather.6.cloned.1.call-done = bf16[32,2,1,32,2048]{4,3,2,1,0:T(8,128)(2,1)} async-done(((bf16[8,2,1,32,2048]{4,3,2,1,0:T(8,128)(2,1)}), bf16[32,2,1,32,2048]{4,3,2,1,0:T(8,128)(2,1)}) %all-gather.6.cloned.1.call-update) | async-done | bytes 8388624 | tf_op jit(solution)/shard_map/all_gather | solution.py:134
  133.5 7.7 %fusion.2 = f32[2,8,4,32,256]{4,3,2,1,0:T(8,128)} fusion(bf16[4,8,2,1,32,2048]{5,4,2,1,0,3:T(8,128)(2,1)} %bitcast.184, bf16[2,2048,256]{2,1,0:T(8,128)(2,1)} %param.23), kind=kOutput, calls=%fused_computation.4 | convolution fusion | flops 2147483648 | bytes 12582912 | tf_op jit(solution)/shard_map/setcd,edf->setcf/dot_general | solution.py:138
  141.2 13.5 %convert_bitcast_fusion = bf16[8,2,4,32,2048]{4,3,2,0,1:T(8,128)(2,1)} fusion(bf16[2,256,2048]{2,1,0:T(8,128)(2,1)S(1)} %copy-done, f32[2,8,4,32,256]{4,3,2,1,0:T(8,128)} %fusion.2, bf16[2,2048,256]{2,1,0:T(8,128)(2,1)} %param.24, bf16[4,8,2,1,32,2048]{5,4,2,1,0,3:T(8,128)(2,1)} %bitcast.185), kind=kOutput, calls=%fused_computation.6 | convolution fusion | flops 4302307328 | bytes 23068672 | tf_op jit(solution)/shard_map/setcf,efd->setcd/dot_general | solution.py:143
  154.7 0.9 copy-done.2
  155.7 3.6 collective-permute-start
  159.4 0.3 broadcast_and_fusion
  159.7 2.8 reshape.401
  162.7 0.6 dynamic-slice
  163.5 2.1 fusion.7
  165.7 1.1 fusion.6
  166.7 0.8 copy-done.1
  167.6 140.2 %all-reduce.3.cloned.1.call-done = bf16[8,2,4,32,2048]{4,3,2,0,1:T(8,128)(2,1)} async-done(((bf16[8,2,4,32,2048]{4,3,2,0,1:T(8,128)(2,1)}), bf16[8,2,4,32,2048]{4,3,2,0,1:T(8,128)(2,1)}) %all-reduce.3.cloned.1.call-update) | async-done | bytes 8388624
  307.8 2.4 constant_dynamic-slice_fusion
  310.2 1.4 copy.70
  311.6 5.5 %all-to-all-start.1 = ((bf16[8,2,1,32,2048]{4,3,2,1,0:T(8,128)(2,1)}), bf16[8,2,1,32,2048]{4,3,2,1,0:T(8,128)(2,1)}, u32[]{:S(2)}, u32[]{:S(2)}) async-start(bf16[8,2,1,32,2048]{4,3,2,1,0:T(8,128)(2,1)} %copy.70), calls=%async_computation.1 | async-start | bytes 4194304 | tf_op jit(solution)/shard_map/all_to_all | solution.py:149
  317.2 3.4 fusion.29
  320.6 0.3 copy.61
  320.9 0.9 copy.103
  322.7 22.5 %all-gather.4.cloned.1.call-done = bf16[1024,1024]{0,1:T(8,128)(2,1)} async-done(((bf16[1024,256]{0,1:T(8,128)(2,1)}), bf16[1024,1024]{0,1:T(8,128)(2,1)}) %all-gather.4.cloned.1.call-update) | async-done | bytes 2097168 | tf_op jit(solution)/shard_map/all_gather | solution.py:116
  345.1 4.1 %convolution_convert_fusion = bf16[1024,512]{1,0:T(8,128)(2,1)} fusion(bf16[1024,1024]{0,1:T(8,128)(2,1)} %all-gather.4.cloned.1.call-done, bf16[1024,512]{1,0:T(8,128)(2,1)} %param.17), kind=kOutput, calls=%fused_computation.28 | convolution fusion | flops 1074266112 | bytes 4194304 | tf_op jit(solution)/shard_map/dot_general | solution.py:115
  349.3 15.9 %all-to-all-done.1 = bf16[8,2,1,32,2048]{4,3,2,1,0:T(8,128)(2,1)} async-done(((bf16[8,2,1,32,2048]{4,3,2,1,0:T(8,128)(2,1)}), bf16[8,2,1,32,2048]{4,3,2,1,0:T(8,128)(2,1)}, u32[]{:S(2)}, u32[]{:S(2)}) %all-to-all-start.1) | async-done | bytes 2097184 | tf_op jit(solution)/shard_map/all_to_all | solution.py:149
  365.2 5.2 %gather_fusion = bf16[256,2048]{1,0:T(8,128)(2,1)} fusion(bf16[512,2048]{1,0:T(8,128)(2,1)} %bitcast.39, s32[1024]{0:T(1024)S(1)} %pad_clamp_fusion), kind=kCustom, calls=%fused_computation | custom fusion | bytes 2098176 | tf_op jit(solution)/shard_map/gather | solution.py:151
  370.4 3.4 reshape.378
  373.8 5.6 %multiply_reduce_fusion = bf16[128,2048]{1,0:T(8,128)(2,1)} fusion(f32[128,2,2048]{2,1,0:T(2,128)} %reshape.378, f32[128,2]{1,0:T(8,128)S(1)} %copy.62), kind=kLoop, calls=%fused_computation.26 | loop fusion | flops 786432 | bytes 2622464 | tf_op jit(solution)/shard_map/reduce_sum | solution.py:154
  (67 shorter events, 2.5 us)
Async XLA Ops:
  7.2 134.0 %copy-start = (bf16[2,256,2048]{2,1,0:T(8,128)(2,1)S(1)}, bf16[2,256,2048]{2,1,0:T(8,128)(2,1)}, u32[]{:S(2)}) copy-start(bf16[2,256,2048]{2,1,0:T(8,128)(2,1)} %param.25) | copy-start | bytes 6291460
  7.2 126.4 %all-gather.6.cloned.1.call-start = ((), (), s32[]{:S(2)}) async-start(), calls=%async_computation.3 | async-start | bytes 10485760 | tf_op jit(solution)/shard_map/all_gather | solution.py:134
  76.1 231.7 %all-reduce.3.cloned.1.call-start = ((), (), s32[]{:S(2)}) async-start(), calls=%async_computation.4 | async-start | bytes 16777216
  154.7 0.9 copy-start.2
  154.7 1.0 copy-start.3
  155.6 7.0 %copy-start.7 = (u32[32]{0:T(128)S(1)}, u32[32]{0:T(128)}, u32[]{:S(2)}) copy-start(u32[32]{0:T(128)} %constant.75) | copy-start | bytes 388
  155.7 7.6 %collective-permute-start = (bf16[2,128,64]{1,2,0:T(8,128)(2,1)S(1)}, bf16[2,128,64]{1,2,0:T(8,128)(2,1)S(1)}, u32[]{:S(2)}, u32[]{:S(2)}) collective-permute-start(bf16[2,128,64]{1,2,0:T(8,128)(2,1)S(1)} %pad_maximum_fusion.2), channel_id=1, source_target_pairs={{0,4},{4,8},{8,12},{12,16},{16,20},{20,24},{24,28},{1,5},{5,9},{9,... | collective-permute-start | bytes 98312 | tf_op jit(solution)/shard_map/ppermute | solution.py:15
  163.4 2.2 copy-start.6
  165.6 1.9 copy-start.1
  311.6 53.5 %all-to-all-start.1 = ((bf16[8,2,1,32,2048]{4,3,2,1,0:T(8,128)(2,1)}), bf16[8,2,1,32,2048]{4,3,2,1,0:T(8,128)(2,1)}, u32[]{:S(2)}, u32[]{:S(2)}) async-start(bf16[8,2,1,32,2048]{4,3,2,1,0:T(8,128)(2,1)} %copy.70), calls=%async_computation.1 | async-start | bytes 4194304 | tf_op jit(solution)/shard_map/all_to_all | solution.py:149
  317.1 28.0 %all-gather.4.cloned.1.call-start = ((), (), s32[]{:S(2)}) async-start(), calls=%async_computation.2 | async-start | bytes 2621440 | tf_op jit(solution)/shard_map/all_gather | solution.py:116
  320.6 1.3 copy-start.4
  320.6 1.6 copy-start.5
Sparse Core Ops, SparseCore 0:
  76.2 57.2 all-gather.5
  154.8 152.9 all-reduce.2
  322.0 23.1 all-gather.3
